TPU v7x, 32 devices: a whole 2x2x4 slice. The times are simulated.
32 devices in a mesh: grp: 2 (over y), fs: 4 (over z), tp: 4 (over x, core).
Axes of the slice: x: 2, y: 2, z: 4, core: 2. Of those that a mesh axis runs over, the one named last changes fastest.
Arguments:
- tokens: bfloat16 [2048, 4096], P(('grp', 'tp')), parts along dimension 0, may hold values from -6 to 6
- routes: int32 [2048, 2], P(('grp', 'tp')), parts along dimension 0, may hold values from 0 to 7, all different within a row; in each aligned block of 256 rows (0 to 255, 256 to 511, ...) at most 128 rows name the same one
- route_weight: float32 [2048, 2], P(('grp', 'tp')), parts along dimension 0, may hold values from 0.2 to 1
- norm_gain: float32 [4096], P('fs'), may hold values from 0.1 to 1.9
- gate_train: float32 [8, 4096, 2048], P(None, 'fs', 'tp'), may hold values from -0.09375 to 0.09375
- up_train: float32 [8, 4096, 2048], P(None, 'fs', 'tp'), may hold values from -0.09375 to 0.09375
- down_train: float32 [8, 2048, 4096], P(None, 'fs', 'tp'), may hold values from -0.125 to 0.125
Outputs:
- gate_serve: bfloat16 [16, 4096, 2048], P(('grp', 'tp'), None, 'fs'), parts along dimension 0
- up_serve: bfloat16 [16, 4096, 2048], P(('grp', 'tp'), None, 'fs'), parts along dimension 0
- down_serve: bfloat16 [16, 2048, 4096], P(('grp', 'tp'), 'fs'), parts along dimension 0
- moe_out: bfloat16 [2048, 4096], P(('grp', 'tp'), 'fs'), parts along dimension 0
There are 2 independent parts, one for each index of `grp`. A program takes and returns all parts, laid end to end along the dimension named above; an argument that names none is the same for every part. Nothing has to cross between parts.
Inputs may be any that keep to these rules, and one draw needn't show every extreme that they name: `routes`: within the 256 rows of each device (aligned blocks), no expert is named by more than 128 rows, a bound that some block reaches; the two experts of a row differ; every expert is named somewhere.
All inputs are finite; a program needn't handle non-finite values.
Results may differ from a plain program's by a relative error of at most 0.0076.
Values may be sent and summed in bfloat16 or wider, within the bound.
A program may use at most 192 MiB of HBM per device.

v0:
```python
import jax
import jax.numpy as jnp
from jax import lax
from jax.sharding import PartitionSpec as P

EXPERTS = 8
CAP = 128


def per_device(tokens, routes, route_weight, norm_gain, gate_train, up_train, down_train):
    gate_cast = (norm_gain[None, :, None] * gate_train).astype(jnp.bfloat16)
    up_cast = (norm_gain[None, :, None] * up_train).astype(jnp.bfloat16)
    down_cast = down_train.astype(jnp.bfloat16)
    gate_mid, up_mid, down_serve = (
        lax.all_to_all(gate_cast, "tp", split_axis=0, concat_axis=2, tiled=True),
        lax.all_to_all(up_cast, "tp", split_axis=0, concat_axis=2, tiled=True),
        lax.all_to_all(down_cast, "tp", split_axis=0, concat_axis=2, tiled=True),
    )
    gate_serve, up_serve = (
        lax.all_to_all(gate_mid, "fs", split_axis=2, concat_axis=1, tiled=True),
        lax.all_to_all(up_mid, "fs", split_axis=2, concat_axis=1, tiled=True),
    )
    tok_rows = tokens.shape[0]
    flat = routes.reshape(-1)
    expert_ids = jnp.arange(EXPERTS, dtype=jnp.int32)
    onehot = (flat[:, None] == expert_ids[None, :]).astype(jnp.int32)
    before = jnp.cumsum(onehot, axis=0) - onehot
    slot = jnp.sum(before * onehot, axis=1)
    place = (flat * CAP + slot).reshape(tok_rows, 2)
    slot_ids = jnp.arange(EXPERTS * CAP, dtype=jnp.int32)
    select = jnp.any(place[None, :, :] == slot_ids[:, None, None], axis=2).astype(jnp.bfloat16)
    outgoing = jnp.dot(select, tokens, preferred_element_type=jnp.float32).astype(jnp.bfloat16)
    arrived = lax.all_to_all(outgoing, "tp", split_axis=0, concat_axis=0, tiled=True)
    senders = lax.axis_size("tp")
    local = gate_serve.shape[0]
    arrived = arrived.reshape(senders, local, CAP, arrived.shape[1])
    gate_h = jnp.einsum("tlcd,ldf->tlcf", arrived, gate_serve, preferred_element_type=jnp.float32)
    up_h = jnp.einsum("tlcd,ldf->tlcf", arrived, up_serve, preferred_element_type=jnp.float32)
    hidden = (jax.nn.silu(gate_h) * up_h).astype(jnp.bfloat16)
    down_cols = lax.all_to_all(down_serve, "fs", split_axis=2, concat_axis=1, tiled=True)
    empty = jnp.zeros((down_cols.shape[2], senders * local * CAP), jnp.float32)
    term = jnp.einsum(
        "tlcf,lfd->dtlc",
        lax.all_gather(hidden, "fs", axis=3, tiled=True),
        down_cols,
        preferred_element_type=jnp.float32,
    )
    summed = term.reshape(empty.shape)
    returned = lax.all_to_all(
        summed.astype(jnp.bfloat16), "tp", split_axis=1, concat_axis=1, tiled=True
    )
    picked = jnp.take(returned, place, axis=1)
    mixed = (
        picked[:, :, 0].astype(jnp.float32) * route_weight[None, :, 0]
        + picked[:, :, 1].astype(jnp.float32) * route_weight[None, :, 1]
    )
    moe_out = mixed.T.astype(jnp.bfloat16)
    return (gate_serve, up_serve, down_serve, moe_out)


def solution(mesh):
    return jax.shard_map(
        per_device,
        mesh=mesh,
        in_specs=(
            P(("grp", "tp"), None),
            P(("grp", "tp"), None),
            P(("grp", "tp"), None),
            P("fs"),
            P(None, "fs", "tp"),
            P(None, "fs", "tp"),
            P(None, "fs", "tp"),
        ),
        out_specs=(
            P(("grp", "tp"), None, "fs"),
            P(("grp", "tp"), None, "fs"),
            P(("grp", "tp"), "fs", None),
            P(("grp", "tp"), "fs"),
        ),
        check_vma=False,
    )
```

profile of v0, /device:TPU:0, one launch (start us, length us, event | category | flops | bytes accessed | tf_op | source)
XLA Modules:
  0.0 1133.6 jit_solution(945579070629410904)
XLA Ops:
  23.4 17.0 %multiply_convert_fusion = (bf16[8,1024,512]{2,1,0:T(8,128)(2,1)}, bf16[8,1024,512]{2,1,0:T(8,128)(2,1)}) fusion(f32[8,1024,512]{2,1,0:T(8,128)} %param.12, f32[1024]{0:T(1024)S(1)} %copy-done.3, f32[8,1024,512]{2,1,0:T(8,128)} %param.11), kind=kLoop, calls=%fused_computation.1 | loop fusion | flops 16777216 | bytes 50335744 | tf_op jit(solution)/shard_map/convert_element_type | solution.py:12
  40.4 76.8 %all-to-all-done.5 = bf16[4,256,4096]{2,1,0:T(8,128)(2,1)} async-done(((bf16[4,256,4096]{2,1,0:T(8,128)(2,1)}), bf16[4,256,4096]{2,1,0:T(8,128)(2,1)}, u32[]{:S(2)}, u32[]{:S(2)}) %all-to-all-start.5) | async-done | bytes 8388640 | tf_op jit(solution)/shard_map/all_to_all | solution.py:33
  117.2 100.5 %all_to_all.126 = bf16[8,1024,512]{2,1,0:T(8,128)(2,1)} all-to-all(bf16[8,1024,512]{2,1,0:T(8,128)(2,1)} %get-tuple-element.30), channel_id=1, replica_groups=mesh['grp'=2,'fs'=4,'tp'=4] {'tp'}, dimensions={0} | all-to-all | bytes 16777216 | tf_op jit(solution)/shard_map/all_to_all | solution.py:16
  223.4 9.1 convert_element_type.53
  232.5 84.1 %all-to-all-done = bf16[8,1024,512]{2,1,0:T(8,128)(2,1)} async-done(((bf16[8,1024,512]{2,1,0:T(8,128)(2,1)}), bf16[8,1024,512]{2,1,0:T(8,128)(2,1)}, u32[]{:S(2)}, u32[]{:S(2)}) %all-to-all-start) | async-done | bytes 8388640 | tf_op jit(solution)/shard_map/all_to_all | solution.py:15
  322.1 11.4 %copy.99 = bf16[2,1024,4,512]{1,3,2,0:T(8,128)(2,1)} copy(bf16[2,1024,4,512]{3,1,0,2:T(8,128)(2,1)} %bitcast.96) | data formatting | bytes 16777216 | tf_op jit(solution)/shard_map/all_to_all | solution.py:16
  333.5 16.4 %copy.100 = bf16[2,1024,2048]{1,0,2:T(2,128)(2,1)} copy(bf16[2,1024,2048]{1,2,0:T(8,128)(2,1)} %bitcast.97) | data formatting | bytes 16777216 | tf_op jit(solution)/shard_map/all_to_all | solution.py:16
  349.9 65.4 %all-to-all-done.4 = bf16[8,512,1024]{2,1,0:T(8,128)(2,1)} async-done(((bf16[8,512,1024]{2,1,0:T(8,128)(2,1)}), bf16[8,512,1024]{2,1,0:T(8,128)(2,1)}, u32[]{:S(2)}, u32[]{:S(2)}) %all-to-all-start.4) | async-done | bytes 8388640 | tf_op jit(solution)/shard_map/all_to_all | solution.py:17
  421.0 11.4 %copy.95 = bf16[2,1024,4,512]{1,3,2,0:T(8,128)(2,1)} copy(bf16[2,1024,4,512]{3,1,0,2:T(8,128)(2,1)} %bitcast.1) | data formatting | bytes 16777216 | tf_op jit(solution)/shard_map/all_to_all | solution.py:15
  432.3 16.4 %copy.96 = bf16[2,1024,2048]{1,0,2:T(2,128)(2,1)} copy(bf16[2,1024,2048]{1,2,0:T(8,128)(2,1)} %bitcast.98) | data formatting | bytes 16777216 | tf_op jit(solution)/shard_map/all_to_all | solution.py:15
  448.7 156.0 %all-to-all-done.3 = bf16[2,1024,2048]{1,0,2:T(2,128)(2,1)} async-done(((bf16[2,1024,2048]{1,0,2:T(2,128)(2,1)}), bf16[2,1024,2048]{1,0,2:T(2,128)(2,1)}, u32[]{:S(2)}, u32[]{:S(2)}) %all-to-all-start.3) | async-done | bytes 8388640 | tf_op jit(solution)/shard_map/all_to_all | solution.py:21
  610.4 21.1 %copy.103 = bf16[4,2,512,1024]{2,1,3,0:T(2,128)(2,1)} copy(bf16[4,2,512,1024]{3,2,1,0:T(8,128)(2,1)} %bitcast.11) | data formatting | bytes 16777216 | tf_op jit(solution)/shard_map/all_to_all | solution.py:17
  631.5 161.5 %all-to-all-done.1 = bf16[2,1024,2048]{1,0,2:T(2,128)(2,1)} async-done(((bf16[2,1024,2048]{1,0,2:T(2,128)(2,1)}), bf16[2,1024,2048]{1,0,2:T(2,128)(2,1)}, u32[]{:S(2)}, u32[]{:S(2)}) %all-to-all-start.1) | async-done | bytes 8388640 | tf_op jit(solution)/shard_map/all_to_all | solution.py:20
  798.8 9.4 copy.101
  808.2 11.4 %copy.102 = bf16[2,4,1024,512]{3,2,1,0:T(8,128)(2,1)} copy(bf16[2,4,1024,512]{2,3,1,0:T(8,128)(2,1)} %bitcast.99) | data formatting | bytes 16777216 | tf_op jit(solution)/shard_map/all_to_all | solution.py:21
  819.6 9.3 copy.97
  828.9 12.2 %copy.98 = bf16[2,4,1024,512]{2,1,3,0:T(4,128)(2,1)} copy(bf16[2,4,1024,512]{2,3,1,0:T(8,128)(2,1)} %bitcast.93) | data formatting | bytes 16777216 | tf_op jit(solution)/shard_map/all_to_all | solution.py:20
  841.1 14.4 %reshape.71 = bf16[2,4096,512,1]{1,2,0,3:T(8,128)(2,1)} reshape(bf16[2,4,1024,512]{2,1,3,0:T(4,128)(2,1)} %copy.98) | data formatting | bytes 16777216 | tf_op jit(solution)/shard_map/all_to_all | solution.py:20
  855.5 10.3 fusion.2
  874.4 174.2 %all-to-all-done.6 = bf16[2,512,4096]{1,0,2:T(2,128)(2,1)} async-done(((bf16[2,512,4096]{1,0,2:T(2,128)(2,1)}), bf16[2,512,4096]{1,0,2:T(2,128)(2,1)}, u32[]{:S(2)}, u32[]{:S(2)}) %all-to-all-start.6) | async-done | bytes 8388640 | tf_op jit(solution)/shard_map/all_to_all | solution.py:40
  1048.6 21.0 %copy.110 = bf16[2,512,4,1024]{3,1,2,0:T(8,128)(2,1)} copy(bf16[2,512,4,1024]{1,0,3,2:T(2,128)(2,1)} %bitcast.23) | data formatting | bytes 16777216 | tf_op jit(solution)/shard_map/all_to_all | solution.py:40
  1069.6 9.2 convert_bitcast_fusion
  1085.7 21.0 %copy.116 = bf16[2,512,4096]{2,1,0:T(8,128)(2,1)} copy(bf16[2,512,4096]{1,0,2:T(2,128)(2,1)} %bitcast.92) | data formatting | bytes 16777216
  1106.7 11.4 %copy.123 = bf16[2,4,1024,512]{3,2,1,0:T(8,128)(2,1)} copy(bf16[2,4,1024,512]{2,3,1,0:T(8,128)(2,1)} %bitcast.94) | data formatting | bytes 16777216
  (52 shorter events, 68.6 us)
Async XLA Ops:
  7.2 4.7 copy-start
  17.6 5.8 copy-start.3
  17.6 99.6 %all-to-all-start.5 = ((bf16[4,256,4096]{2,1,0:T(8,128)(2,1)}), bf16[4,256,4096]{2,1,0:T(8,128)(2,1)}, u32[]{:S(2)}, u32[]{:S(2)}) async-start(bf16[4,256,4096]{2,1,0:T(8,128)(2,1)} %bitcast.95), calls=%async_computation.5 | async-start | bytes 16777216 | tf_op jit(solution)/shard_map/all_to_all | solution.py:33
  217.7 98.8 %all-to-all-start = ((bf16[8,1024,512]{2,1,0:T(8,128)(2,1)}), bf16[8,1024,512]{2,1,0:T(8,128)(2,1)}, u32[]{:S(2)}, u32[]{:S(2)}) async-start(bf16[8,1024,512]{2,1,0:T(8,128)(2,1)} %get-tuple-element.31), calls=%async_computation | async-start | bytes 16777216 | tf_op jit(solution)/shard_map/all_to_all | solution.py:15
  316.5 98.8 %all-to-all-start.4 = ((bf16[8,512,1024]{2,1,0:T(8,128)(2,1)}), bf16[8,512,1024]{2,1,0:T(8,128)(2,1)}, u32[]{:S(2)}, u32[]{:S(2)}) async-start(bf16[8,512,1024]{2,1,0:T(8,128)(2,1)} %convert_element_type.53), calls=%async_computation.4 | async-start | bytes 16777216 | tf_op jit(solution)/shard_map/all_to_all | solution.py:17
  415.3 189.4 %all-to-all-start.3 = ((bf16[2,1024,2048]{1,0,2:T(2,128)(2,1)}), bf16[2,1024,2048]{1,0,2:T(2,128)(2,1)}, u32[]{:S(2)}, u32[]{:S(2)}) async-start(bf16[2,1024,2048]{1,0,2:T(2,128)(2,1)} %copy.100), calls=%async_computation.3 | async-start | bytes 16777216 | tf_op jit(solution)/shard_map/all_to_all | solution.py:21
  604.7 188.2 %all-to-all-start.1 = ((bf16[2,1024,2048]{1,0,2:T(2,128)(2,1)}), bf16[2,1024,2048]{1,0,2:T(2,128)(2,1)}, u32[]{:S(2)}, u32[]{:S(2)}) async-start(bf16[2,1024,2048]{1,0,2:T(2,128)(2,1)} %copy.96), calls=%async_computation.1 | async-start | bytes 16777216 | tf_op jit(solution)/shard_map/all_to_all | solution.py:20
  792.9 255.7 %all-to-all-start.6 = ((bf16[2,512,4096]{1,0,2:T(2,128)(2,1)}), bf16[2,512,4096]{1,0,2:T(2,128)(2,1)}, u32[]{:S(2)}, u32[]{:S(2)}) async-start(bf16[2,512,4096]{1,0,2:T(2,128)(2,1)} %bitcast.91), calls=%async_computation.6 | async-start | bytes 16777216 | tf_op jit(solution)/shard_map/all_to_all | solution.py:40
  798.6 271.1 %all-gather.2.cloned.1.call-start = ((), (), s32[]{:S(2)}) async-start(), calls=%async_computation.8 | async-start | bytes 5242880 | tf_op jit(solution)/shard_map/all_gather | solution.py:44
  855.5 10.4 copy-start.2
  1078.8 6.3 copy-start.7
  1080.3 37.8 %all-to-all-start.7 = ((bf16[1024,4,256]{0,2,1:T(8,128)(2,1)}), bf16[1024,4,256]{0,2,1:T(8,128)(2,1)}, u32[]{:S(2)}, u32[]{:S(2)}) async-start(bf16[1024,4,256]{0,2,1:T(8,128)(2,1)} %bitcast.29), calls=%async_computation.7 | async-start | bytes 4194304 | tf_op jit(solution)/shard_map/all_to_all | solution.py:49
  1118.1 6.0 copy-start.4
  1118.1 7.6 copy-start.5
  1118.1 7.6 copy-start.6
  1118.1 8.7 copy-start.1
Sparse Core Ops, SparseCore 0:
  874.5 159.5 all-gather.1
where the time goes:
time: 1140 us; the launch traced here: 1130 us
  waiting for transfers between devices  718 us (63%)
  local copies, waits for them, and re-layouts  197 us (17%)
  blocking collectives  101 us (9%)
  starting transfers between devices  38.7 us (3%)
  matrix products  33.8 us (3%)
  other arithmetic  31.7 us (3%)
  between operations  14.3 us (1%)
    all_to_all x1, waiting for transfers between devices, per_device(): lax.all_to_all(down_serve, 'fs', split_axis=2, concat_axis=1, tiled=True)  174 us
    all_to_all x1, waiting for transfers between devices, per_device(): lax.all_to_all(gate_mid, 'fs', split_axis=2, concat_axis=1, tiled=True)  161 us
    all_to_all x1, waiting for transfers between devices, per_device(): lax.all_to_all(up_mid, 'fs', split_axis=2, concat_axis=1, tiled=True)  156 us
    all_to_all x1, blocking collectives, per_device(): lax.all_to_all(up_cast, 'tp', split_axis=0, concat_axis=2, tiled=True)  101 us
    all_to_all x1, waiting for transfers between devices, per_device(): lax.all_to_all(gate_cast, 'tp', split_axis=0, concat_axis=2, tiled=True)  84.1 us
    all_to_all x1, waiting for transfers between devices, per_device(): lax.all_to_all(outgoing, 'tp', split_axis=0, concat_axis=0, tiled=True)  76.8 us
    all_to_all x1, waiting for transfers between devices, per_device(): lax.all_to_all(down_cast, 'tp', split_axis=0, concat_axis=2, tiled=True)  65.4 us
    all_to_all x3, local copies, waits for them, and re-layouts, per_device(): lax.all_to_all(gate_mid, 'fs', split_axis=2, concat_axis=1, tiled=True)  35.8 us
  transfers between devices with their start and end apart: 8, of which 6 were waited for; matrix products, arithmetic and copies ran while one was open for 21% of the time, Pallas kernels for 0%

commit v1 on v0

--- a/solution.py
+++ b/solution.py
@@ -7,12 +7,19 @@
 CAP = 128
 
 
+def swap_blocks(value, axis, split, join):
+    size = lax.axis_size(axis)
+    tiles = jnp.stack(jnp.split(value, size, axis=split), axis=0)
+    tiles = lax.all_to_all(tiles, axis, split_axis=0, concat_axis=0)
+    return jnp.concatenate(tiles, axis=join)
+
+
 def per_device(tokens, routes, route_weight, norm_gain, gate_train, up_train, down_train):
     gate_cast = (norm_gain[None, :, None] * gate_train).astype(jnp.bfloat16)
     up_cast = (norm_gain[None, :, None] * up_train).astype(jnp.bfloat16)
     down_cast = down_train.astype(jnp.bfloat16)
     gate_mid, up_mid, down_serve = (
-        lax.all_to_all(gate_cast, "tp", split_axis=0, concat_axis=2, tiled=True),
+        swap_blocks(gate_cast, "tp", 0, 2),
         lax.all_to_all(up_cast, "tp", split_axis=0, concat_axis=2, tiled=True),
         lax.all_to_all(down_cast, "tp", split_axis=0, concat_axis=2, tiled=True),
     )

time: 1140 us -> 1160 us (1.018)
    all_to_all x2 -> x1, local copies, waits for them, and re-layouts: 27.7 us -> 7.76 us  [swap_blocks(): tiles = lax.all_to_all(tiles, axis, split_axis=0, concat_axis=0)]
    reshape x0 -> x1, local copies, waits for them, and re-layouts: none -> 16.4 us  [swap_blocks(): return jnp.concatenate(tiles, axis=join)]
    another operation x1 -> x3, local copies, waits for them, and re-layouts: 0.01 us -> 12.1 us  [the longest x2 12 us: swap_blocks(): tiles = jnp.stack(jnp.split(value, size, axis=split), axis=0)]
    unnamed x19 -> x17, local copies, waits for them, and re-layouts: 33.4 us -> 32.6 us
  transfers between devices with their start and end apart: 8 -> 8, of which waited for: 6 -> 6; matrix products, arithmetic and copies ran while one was open for 21% -> 19% of each run, Pallas kernels for 0% -> 0%
where the time goes in v1:
time: 1160 us; the launch traced here: 1150 us
  waiting for transfers between devices  728 us (63%)
  local copies, waits for them, and re-layouts  204 us (18%)
  blocking collectives  101 us (9%)
  starting transfers between devices  38.7 us (3%)
  matrix products  35.7 us (3%)
  other arithmetic  33 us (3%)
  between operations  14.3 us (1%)
    all_to_all x1, waiting for transfers between devices, per_device(): lax.all_to_all(down_serve, 'fs', split_axis=2, concat_axis=1, tiled=True)  172 us
    all_to_all x1, waiting for transfers between devices, per_device(): lax.all_to_all(up_mid, 'fs', split_axis=2, concat_axis=1, tiled=True)  162 us
    all_to_all x1, waiting for transfers between devices, per_device(): lax.all_to_all(gate_mid, 'fs', split_axis=2, concat_axis=1, tiled=True)  156 us
    all_to_all x1, blocking collectives, per_device(): lax.all_to_all(outgoing, 'tp', split_axis=0, concat_axis=0, tiled=True)  101 us
    all_to_all x1, waiting for transfers between devices, swap_blocks(): tiles = lax.all_to_all(tiles, axis, split_axis=0, concat_axis=0)  84.9 us
    all_to_all x1, waiting for transfers between devices, per_device(): lax.all_to_all(up_cast, 'tp', split_axis=0, concat_axis=2, tiled=True)  84.1 us
    all_to_all x1, waiting for transfers between devices, per_device(): lax.all_to_all(down_cast, 'tp', split_axis=0, concat_axis=2, tiled=True)  69 us
    all_to_all x3, local copies, waits for them, and re-layouts, per_device(): lax.all_to_all(gate_mid, 'fs', split_axis=2, concat_axis=1, tiled=True)  35.8 us
  transfers between devices with their start and end apart: 8, of which 6 were waited for; matrix products, arithmetic and copies ran while one was open for 19% of the time, Pallas kernels for 0%

profile of v1, /device:TPU:0, one launch (start us, length us, event | category | flops | bytes accessed | tf_op | source)
XLA Modules:
  0.0 1154.4 jit_solution(17331748421417549773)
XLA Ops:
  7.2 15.1 %multiply_convert_fusion = (bf16[8,1024,512]{2,1,0:T(8,128)(2,1)}, bf16[8,1024,512]{2,1,0:T(8,128)(2,1)S(1)}) fusion(f32[8,1024,512]{2,1,0:T(8,128)} %param.12, f32[1024]{0:T(1024)} %param.10, f32[8,1024,512]{2,1,0:T(8,128)} %param.11), kind=kLoop, calls=%fused_computation.1 | loop fusion | flops 16777216 | bytes 50335744 | tf_op jit(solution)/shard_map/convert_element_type | solution.py:19
  26.8 11.4 copy.131
  52.9 84.9 %all-to-all-done = bf16[4,2,1024,512]{2,3,1,0:T(8,128)(2,1)} async-done(((bf16[4,2,1024,512]{2,3,1,0:T(8,128)(2,1)}), bf16[4,2,1024,512]{2,3,1,0:T(8,128)(2,1)}, u32[]{:S(2)}, u32[]{:S(2)}) %all-to-all-start) | async-done | bytes 8388640 | tf_op jit(solution)/shard_map/all_to_all | solution.py:13
  137.8 100.6 %all_to_all.113 = bf16[4,256,4096]{2,1,0:T(8,128)(2,1)} all-to-all(bf16[4,256,4096]{2,1,0:T(8,128)(2,1)} %bitcast.102), channel_id=1, replica_groups=mesh['grp'=2,'fs'=4,'tp'=4] {'tp'}, dimensions={0} | all-to-all | bytes 16777216 | tf_op jit(solution)/shard_map/all_to_all | solution.py:40
  253.1 84.1 %all-to-all-done.2 = bf16[8,1024,512]{2,1,0:T(8,128)(2,1)} async-done(((bf16[8,1024,512]{2,1,0:T(8,128)(2,1)}), bf16[8,1024,512]{2,1,0:T(8,128)(2,1)}, u32[]{:S(2)}, u32[]{:S(2)}) %all-to-all-start.2) | async-done | bytes 8388640 | tf_op jit(solution)/shard_map/all_to_all | solution.py:23
  350.6 16.4 %copy.133 = bf16[2,1024,2048]{1,0,2:T(2,128)(2,1)} copy(bf16[2,1024,2048]{1,2,0:T(8,128)(2,1)} %bitcast.103) | data formatting | bytes 16777216 | tf_op jit(solution)/shard_map/reshape | solution.py:14
  367.0 69.0 %all-to-all-done.4 = bf16[8,512,1024]{2,1,0:T(8,128)(2,1)} async-done(((bf16[8,512,1024]{2,1,0:T(8,128)(2,1)}), bf16[8,512,1024]{2,1,0:T(8,128)(2,1)}, u32[]{:S(2)}, u32[]{:S(2)}) %all-to-all-start.4) | async-done | bytes 8388640 | tf_op jit(solution)/shard_map/all_to_all | solution.py:24
  441.6 11.4 copy.136
  453.0 16.4 %copy.137 = bf16[2,1024,2048]{1,0,2:T(2,128)(2,1)} copy(bf16[2,1024,2048]{1,2,0:T(8,128)(2,1)} %bitcast.104) | data formatting | bytes 16777216 | tf_op jit(solution)/shard_map/all_to_all | solution.py:23
  469.4 156.0 %all-to-all-done.1 = bf16[2,1024,2048]{1,0,2:T(2,128)(2,1)} async-done(((bf16[2,1024,2048]{1,0,2:T(2,128)(2,1)}), bf16[2,1024,2048]{1,0,2:T(2,128)(2,1)}, u32[]{:S(2)}, u32[]{:S(2)}) %all-to-all-start.1) | async-done | bytes 8388640 | tf_op jit(solution)/shard_map/all_to_all | solution.py:27
  631.1 21.1 %copy.140 = bf16[4,2,512,1024]{2,1,3,0:T(2,128)(2,1)} copy(bf16[4,2,512,1024]{3,2,1,0:T(8,128)(2,1)} %bitcast.14) | data formatting | bytes 16777216 | tf_op jit(solution)/shard_map/all_to_all | solution.py:24
  652.2 161.5 %all-to-all-done.3 = bf16[2,1024,2048]{1,0,2:T(2,128)(2,1)} async-done(((bf16[2,1024,2048]{1,0,2:T(2,128)(2,1)}), bf16[2,1024,2048]{1,0,2:T(2,128)(2,1)}, u32[]{:S(2)}, u32[]{:S(2)}) %all-to-all-start.3) | async-done | bytes 8388640 | tf_op jit(solution)/shard_map/all_to_all | solution.py:28
  819.6 9.3 copy.134
  828.8 12.2 %copy.135 = bf16[2,4,1024,512]{2,1,3,0:T(4,128)(2,1)} copy(bf16[2,4,1024,512]{2,3,1,0:T(8,128)(2,1)} %bitcast.100) | data formatting | bytes 16777216 | tf_op jit(solution)/shard_map/all_to_all | solution.py:27
  841.0 14.3 %reshape.79 = bf16[2,4096,512,1]{1,2,0,3:T(8,128)(2,1)} reshape(bf16[2,4,1024,512]{2,1,3,0:T(4,128)(2,1)} %copy.135) | data formatting | bytes 16777216 | tf_op jit(solution)/shard_map/all_to_all | solution.py:27
  855.3 9.4 copy.138
  864.8 11.4 copy.139
  876.2 10.2 fusion.2
  886.4 10.6 fusion.5
  897.0 172.4 %all-to-all-done.6 = bf16[2,512,4096]{1,0,2:T(2,128)(2,1)} async-done(((bf16[2,512,4096]{1,0,2:T(2,128)(2,1)}), bf16[2,512,4096]{1,0,2:T(2,128)(2,1)}, u32[]{:S(2)}, u32[]{:S(2)}) %all-to-all-start.6) | async-done | bytes 8388640 | tf_op jit(solution)/shard_map/all_to_all | solution.py:47
  1069.4 21.0 %copy.147 = bf16[2,512,4,1024]{3,1,2,0:T(8,128)(2,1)} copy(bf16[2,512,4,1024]{1,0,3,2:T(2,128)(2,1)} %bitcast.26) | data formatting | bytes 16777216 | tf_op jit(solution)/shard_map/all_to_all | solution.py:47
  1090.4 9.2 convert_bitcast_fusion
  1106.5 21.0 %copy.153 = bf16[2,512,4096]{2,1,0:T(8,128)(2,1)} copy(bf16[2,512,4096]{1,0,2:T(2,128)(2,1)} %bitcast.99) | data formatting | bytes 16777216
  1127.5 11.4 copy.160
  (53 shorter events, 80.0 us)
Async XLA Ops:
  7.2 39.9 %copy-start = (bf16[256,4096]{1,0:T(8,128)(2,1)S(1)}, bf16[256,4096]{1,0:T(8,128)(2,1)}, u32[]{:S(2)}) copy-start(bf16[256,4096]{1,0:T(8,128)(2,1)} %param.7) | copy-start | bytes 6291460
  38.2 5.8 copy-start.2
  38.2 99.6 %all-to-all-start = ((bf16[4,2,1024,512]{2,3,1,0:T(8,128)(2,1)}), bf16[4,2,1024,512]{2,3,1,0:T(8,128)(2,1)}, u32[]{:S(2)}, u32[]{:S(2)}) async-start(bf16[4,2,1024,512]{2,3,1,0:T(8,128)(2,1)} %copy.131), calls=%async_computation | async-start | bytes 16777216 | tf_op jit(solution)/shard_map/all_to_all | solution.py:13
  238.4 98.8 %all-to-all-start.2 = ((bf16[8,1024,512]{2,1,0:T(8,128)(2,1)}), bf16[8,1024,512]{2,1,0:T(8,128)(2,1)}, u32[]{:S(2)}, u32[]{:S(2)}) async-start(bf16[8,1024,512]{2,1,0:T(8,128)(2,1)} %get-tuple-element.38), calls=%async_computation.2 | async-start | bytes 16777216 | tf_op jit(solution)/shard_map/all_to_all | solution.py:23
  337.2 98.8 %all-to-all-start.4 = ((bf16[8,512,1024]{2,1,0:T(8,128)(2,1)}), bf16[8,512,1024]{2,1,0:T(8,128)(2,1)}, u32[]{:S(2)}, u32[]{:S(2)}) async-start(bf16[8,512,1024]{2,1,0:T(8,128)(2,1)} %convert_element_type.53), calls=%async_computation.4 | async-start | bytes 16777216 | tf_op jit(solution)/shard_map/all_to_all | solution.py:24
  436.0 189.5 %all-to-all-start.1 = ((bf16[2,1024,2048]{1,0,2:T(2,128)(2,1)}), bf16[2,1024,2048]{1,0,2:T(2,128)(2,1)}, u32[]{:S(2)}, u32[]{:S(2)}) async-start(bf16[2,1024,2048]{1,0,2:T(2,128)(2,1)} %copy.133), calls=%async_computation.1 | async-start | bytes 16777216 | tf_op jit(solution)/shard_map/all_to_all | solution.py:27
  625.4 188.3 %all-to-all-start.3 = ((bf16[2,1024,2048]{1,0,2:T(2,128)(2,1)}), bf16[2,1024,2048]{1,0,2:T(2,128)(2,1)}, u32[]{:S(2)}, u32[]{:S(2)}) async-start(bf16[2,1024,2048]{1,0,2:T(2,128)(2,1)} %copy.137), calls=%async_computation.3 | async-start | bytes 16777216 | tf_op jit(solution)/shard_map/all_to_all | solution.py:28
  813.7 255.7 %all-to-all-start.6 = ((bf16[2,512,4096]{1,0,2:T(2,128)(2,1)}), bf16[2,512,4096]{1,0,2:T(2,128)(2,1)}, u32[]{:S(2)}, u32[]{:S(2)}) async-start(bf16[2,512,4096]{1,0,2:T(2,128)(2,1)} %bitcast.98), calls=%async_computation.6 | async-start | bytes 16777216 | tf_op jit(solution)/shard_map/all_to_all | solution.py:47
  819.3 271.1 %all-gather.2.cloned.1.call-start = ((), (), s32[]{:S(2)}) async-start(), calls=%async_computation.8 | async-start | bytes 5242880 | tf_op jit(solution)/shard_map/all_gather | solution.py:51
  1099.6 6.3 copy-start.6
  1101.1 37.8 %all-to-all-start.7 = ((bf16[1024,4,256]{0,2,1:T(8,128)(2,1)}), bf16[1024,4,256]{0,2,1:T(8,128)(2,1)}, u32[]{:S(2)}, u32[]{:S(2)}) async-start(bf16[1024,4,256]{0,2,1:T(8,128)(2,1)} %bitcast.32), calls=%async_computation.7 | async-start | bytes 4194304 | tf_op jit(solution)/shard_map/all_to_all | solution.py:56
  1138.9 6.0 copy-start.3
  1138.9 7.6 copy-start.4
  1138.9 7.6 copy-start.5
  1138.9 8.7 copy-start.1
Sparse Core Ops, SparseCore 0:
  897.1 159.5 all-gather.1
